TPU v7x, 256 devices: a 4x2x16 block of a 4x16x16 slice. The times are simulated.
256 devices in a mesh: grp: 2 (over y), fs: 16 (over z), tp: 8 (over x, core).
Axes of the slice: x: 4, y: 2, z: 16, core: 2. Of those that a mesh axis runs over, the one named last changes fastest.
The devices are a block of a 4x16x16 slice.
Arguments:
- tokens: bfloat16 [128, 128, 2048], P(('grp', 'fs'), None, 'tp'), parts along dimension 0, may hold values from -100 to 100
- mix_gain: float32 [2048], replicated, may hold values from 0.1 to 1.9
- gate_outer: bfloat16 [2048, 1024], P('fs', 'tp'), may hold values from -0.125 to 0.125
- gate_inner: bfloat16 [2048, 1024], P('fs', 'tp'), may hold values from -0.125 to 0.125
- value_weight: bfloat16 [2048, 1024], P('fs', 'tp'), may hold values from -0.125 to 0.125
- conv_taps: float32 [3, 1024], replicated, may hold values from -3 to 3
- mix_out: bfloat16 [1024, 2048], P('tp', 'fs'), may hold values from -0.25 to 0.25
- ffn_gain: float32 [2048], replicated, may hold values from 0.1 to 1.9
- ffn_gate: bfloat16 [2048, 5632], P('fs', 'tp'), may hold values from -0.125 to 0.125
- ffn_up: bfloat16 [2048, 5632], P('fs', 'tp'), may hold values from -0.125 to 0.125
- ffn_down: bfloat16 [5632, 2048], P('tp', 'fs'), may hold values from -0.109375 to 0.109375
- out_gain: float32 [2048], replicated, may hold values from 0.1 to 1.9
Outputs:
- layer_out: bfloat16 [128, 128, 2048], P(('grp', 'fs'), None, 'tp'), parts along dimension 0
There are 2 independent parts, one for each index of `grp`. A program takes and returns all parts, laid end to end along the dimension named above; an argument that names none is the same for every part. Nothing has to cross between parts.
All inputs are finite; a program needn't handle non-finite values.
Results may differ from a plain program's by a relative error of at most 0.015.
Values may be sent and summed in bfloat16 or wider, within the bound.
No kernel may reach another device: no remote copies, remote signals or barrier semaphores. Data moves between devices by JAX's collectives and lax.ppermute only.
A program may use at most 64 MiB of HBM per device.

v0:
```python
import jax
import jax.numpy as jnp
from jax import lax
from jax.sharding import PartitionSpec as P


def in_order(parts, dim):
    parts = jnp.moveaxis(parts, 0, dim)
    shape = parts.shape
    return parts.reshape(*shape[:dim], shape[dim] * shape[dim + 1], *shape[dim + 2 :])


def copy_for_each(shard, axis):
    copies = jnp.broadcast_to(shard, (lax.axis_size(axis), *shard.shape))
    return lax.all_to_all(copies, axis, split_axis=0, concat_axis=0, tiled=True)


def collect(shard, axis, dim):
    return in_order(copy_for_each(shard, axis), dim)


def side_by_side(arrays, axis, dim, along):
    both = jnp.concatenate(arrays, axis=along)
    filled, at, outs = (lax.all_gather(both, axis, axis=dim, tiled=True), 0, [])
    for a in arrays:
        outs.append(lax.slice_in_dim(filled, at, at + a.shape[along], axis=along))
        at += a.shape[along]
    return tuple(outs)


def in_blocks(shard, dim, count):
    shape = shard.shape
    parts = shard.reshape(*shape[:dim], count, shape[dim] // count, *shape[dim + 1 :])
    return jnp.moveaxis(parts, dim, 0)


def summed_on_arrival(shard, axis, dim):
    parts = in_blocks(shard, dim, lax.axis_size(axis))
    arrived = lax.all_to_all(parts, axis, split_axis=0, concat_axis=0, tiled=True)
    return arrived.astype(jnp.float32).sum(axis=0)


def of_everyone(shard, axis):
    return copy_for_each(shard, axis).sum(axis=0)


def rms_norm(values, gain):
    floats = values.astype(jnp.float32)
    scaled = floats * lax.rsqrt(jnp.mean(floats * floats, axis=-1, keepdims=True) + 1e-06)
    return (scaled * gain).astype(jnp.bfloat16)


def local(
    tokens,
    mix_gain,
    gate_outer,
    gate_inner,
    value_weight,
    conv_taps,
    mix_out,
    ffn_gain,
    ffn_gate,
    ffn_up,
    ffn_down,
    out_gain,
):
    seq_count, length, columns = tokens.shape
    row_count = seq_count * length
    width = columns * lax.axis_size("tp")
    whole = collect(tokens, "tp", 2).reshape(row_count, width)
    normed = rms_norm(whole, mix_gain)
    channels = gate_outer.shape[1]
    pieces = side_by_side((gate_outer, gate_inner, value_weight), "fs", 0, 1)
    sliced = normed
    outer = jnp.dot(sliced, pieces[0], preferred_element_type=jnp.float32)
    inner = jnp.dot(sliced, pieces[1], preferred_element_type=jnp.float32)
    values = jnp.dot(sliced, pieces[2], preferred_element_type=jnp.float32)
    outer = outer.astype(jnp.bfloat16)
    inner = inner.astype(jnp.bfloat16)
    values = values.astype(jnp.bfloat16)
    product = (inner.astype(jnp.float32) * values.astype(jnp.float32)).reshape(
        seq_count, length, channels
    )
    own_taps = lax.dynamic_slice_in_dim(conv_taps, lax.axis_index("tp") * channels, channels, 1)
    tap_count = conv_taps.shape[0]
    padded = jnp.pad(product, ((0, 0), (tap_count - 1, 0), (0, 0)))
    conv = jnp.zeros((seq_count, length, channels), jnp.float32)
    for offset in range(tap_count):
        conv = conv + own_taps[offset] * padded[:, offset : offset + length]
    gated = (outer.astype(jnp.float32) * conv.reshape(row_count, channels)).astype(jnp.bfloat16)
    mix_terms = jnp.dot(gated, collect(mix_out, "fs", 1), preferred_element_type=jnp.float32)
    mix_summed = summed_on_arrival(mix_terms.astype(jnp.bfloat16), "tp", 1)
    first = (tokens.reshape(row_count, columns).astype(jnp.float32) + mix_summed).astype(
        jnp.bfloat16
    )
    whole_ffn = collect(first.reshape(seq_count, length, columns), "tp", 2).reshape(
        row_count, width
    )
    normed_ffn = rms_norm(whole_ffn, ffn_gain)
    pieces = side_by_side((ffn_gate, ffn_up), "fs", 0, 1)
    sliced = normed_ffn
    gate = jnp.dot(sliced, pieces[0], preferred_element_type=jnp.float32)
    upward = jnp.dot(sliced, pieces[1], preferred_element_type=jnp.float32)
    hidden = (jax.nn.silu(gate) * upward).astype(jnp.bfloat16)
    down_terms = jnp.dot(
        hidden,
        lax.all_gather(ffn_down, "fs", axis=1, tiled=True),
        preferred_element_type=jnp.float32,
    )
    down_summed = summed_on_arrival(down_terms.astype(jnp.bfloat16), "tp", 1)
    second = first.astype(jnp.float32) + down_summed
    squares = of_everyone(jnp.sum(second * second, axis=1), "tp")
    factor = lax.rsqrt(squares / width + 1e-06)
    own_gain = lax.dynamic_slice_in_dim(out_gain, lax.axis_index("tp") * columns, columns, 0)
    result = second * factor[:, None] * own_gain
    return result.astype(jnp.bfloat16).reshape(seq_count, length, columns)


def solution(mesh):
    in_specs = (
        P(("grp", "fs"), None, "tp"),
        P(),
        P("fs", "tp"),
        P("fs", "tp"),
        P("fs", "tp"),
        P(),
        P("tp", "fs"),
        P(),
        P("fs", "tp"),
        P("fs", "tp"),
        P("tp", "fs"),
        P(),
    )
    out_specs = P(("grp", "fs"), None, "tp")
    return jax.shard_map(local, mesh=mesh, in_specs=in_specs, out_specs=out_specs, check_vma=False)
```

profile of v0, /device:TPU:33, one launch (start us, length us, event | category | flops | bytes accessed | tf_op | source)
XLA Modules:
  0.0 347.9 jit_solution(9210337294262374817)
XLA Ops:
  8.1 1.8 pad_maximum_fusion
  10.0 2.5 broadcast_in_dim.20
  12.5 24.1 %all-to-all-start = ((bf16[8,4,128,256]{3,2,1,0:T(8,128)(2,1)}), bf16[8,4,128,256]{3,2,1,0:T(8,128)(2,1)S(1)}, u32[]{:S(2)}, u32[]{:S(2)}) async-start(bf16[8,4,128,256]{3,2,1,0:T(8,128)(2,1)} %broadcast_in_dim.20), calls=%async_computation | async-start | bytes 4194304 | tf_op jit(solution)/shard_map/all_to_all | solution.py:15
  36.7 26.1 %all-to-all-done = bf16[8,4,128,256]{3,2,1,0:T(8,128)(2,1)S(1)} async-done(((bf16[8,4,128,256]{3,2,1,0:T(8,128)(2,1)}), bf16[8,4,128,256]{3,2,1,0:T(8,128)(2,1)S(1)}, u32[]{:S(2)}, u32[]{:S(2)}) %all-to-all-start) | async-done | bytes 2097184 | tf_op jit(solution)/shard_map/all_to_all | solution.py:15
  63.7 5.7 %all-to-all-start.1 = ((bf16[16,128,128]{1,2,0:T(8,128)(2,1)}), bf16[16,128,128]{1,2,0:T(8,128)(2,1)S(1)}, u32[]{:S(2)}, u32[]{:S(2)}) async-start(bf16[16,128,128]{1,2,0:T(8,128)(2,1)} %broadcast_in_dim.21), calls=%async_computation.1 | async-start | bytes 1048576 | tf_op jit(solution)/shard_map/all_to_all | solution.py:15
  70.0 2.4 copy.24
  72.4 2.0 copy.33
  75.5 23.0 %all-gather.4.cloned.1.call-done = bf16[2048,384]{1,0:T(8,128)(2,1)} async-done(((bf16[128,384]{1,0:T(8,128)(2,1)}), bf16[2048,384]{1,0:T(8,128)(2,1)}) %all-gather.4.cloned.1.call-update) | async-done | bytes 1572880 | tf_op jit(solution)/shard_map/all_gather | solution.py:24
  98.4 1.7 fusion.14
  100.2 1.8 fusion.13
  102.1 4.7 %convolution_convert_fusion = bf16[512,2048]{1,0:T(8,128)(2,1)} fusion(bf16[128,2048]{0,1:T(8,128)(2,1)S(1)} %bitcast.61, f32[512,128]{1,0:T(8,128)S(1)} %bitcast.63, bf16[512,2048]{1,0:T(8,128)(2,1)S(1)} %multiply_convert_fusion.1, bf16[2048,384]{1,0:T(8,128)(2,1)} %all-gather.4.cloned.1.call-done), kind=kOutput, calls=%fused_computation.10 | convolution fusion | flops 538181632 | bytes 5505024 | tf_op jit(solution)/shard_map/dot_general | solution.py:91
  106.7 3.1 copy.38
  109.8 13.0 %all-to-all-start.2 = ((bf16[8,512,256]{2,1,0:T(8,128)(2,1)}), bf16[8,512,256]{2,1,0:T(8,128)(2,1)S(1)}, u32[]{:S(2)}, u32[]{:S(2)}) async-start(bf16[8,512,256]{2,1,0:T(8,128)(2,1)} %bitcast.53), calls=%async_computation.2 | async-start | bytes 4194304 | tf_op jit(solution)/shard_map/all_to_all | solution.py:39
  123.6 25.4 %all-to-all-done.2 = bf16[8,512,256]{2,1,0:T(8,128)(2,1)S(1)} async-done(((bf16[8,512,256]{2,1,0:T(8,128)(2,1)}), bf16[8,512,256]{2,1,0:T(8,128)(2,1)S(1)}, u32[]{:S(2)}, u32[]{:S(2)}) %all-to-all-start.2) | async-done | bytes 2097184 | tf_op jit(solution)/shard_map/all_to_all | solution.py:39
  149.7 29.7 %all_to_all.31 = bf16[8,4,128,256]{3,2,1,0:T(8,128)(2,1)S(1)} all-to-all(bf16[8,4,128,256]{3,2,1,0:T(8,128)(2,1)S(1)} %broadcast_in_dim.22), channel_id=1, replica_groups=mesh['grp'=2,'fs'=16,'tp'=8] {'tp'}, dimensions={0} | all-to-all | bytes 4194304 | tf_op jit(solution)/shard_map/all_to_all | solution.py:15
  179.9 2.4 copy.27
  182.3 4.0 %copy.34 = f32[64,8,8,256]{3,1,2,0:T(8,128)} copy(f32[64,8,8,256]{3,2,1,0:T(8,128)S(1)} %bitcast.52) | data formatting | bytes 8388608
  186.8 13.6 %all-gather.6.cloned.1.call-done = bf16[2048,1408]{0,1:T(8,128)(2,1)} async-done(((bf16[128,1408]{0,1:T(8,128)(2,1)}), bf16[2048,1408]{0,1:T(8,128)(2,1)}) %all-gather.6.cloned.1.call-update) | async-done | bytes 5767184 | tf_op jit(solution)/shard_map/all_gather | solution.py:24
  200.4 6.0 %fusion.4 = f32[512,704]{0,1:T(8,128)} fusion(bf16[2048,1408]{0,1:T(8,128)(2,1)} %all-gather.6.cloned.1.call-done, f32[512,2048]{1,0:T(8,128)} %bitcast.57, f32[2048]{0:T(1024)S(1)} %copy-done.4, f32[512]{0:T(512)S(1)} %rsqrt_bitcast_fusion.1), kind=kOutput, calls=%fused_computation.14 | convolution fusion | flops 1479540736 | bytes 8529920 | tf_op jit(solution)/shard_map/dot_general | solution.py:102
  206.4 74.6 %all-gather.8.cloned.1.call-done = bf16[704,2048]{1,0:T(8,128)(2,1)} async-done(((bf16[704,128]{1,0:T(8,128)(2,1)}), bf16[704,2048]{1,0:T(8,128)(2,1)}) %all-gather.8.cloned.1.call-update) | async-done | bytes 2883600 | tf_op jit(solution)/shard_map/all_gather | solution.py:107
  281.0 7.8 %convolution_convert_fusion.1 = bf16[512,2048]{1,0:T(8,128)(2,1)S(1)} fusion(bf16[704,2048]{1,0:T(8,128)(2,1)} %all-gather.8.cloned.1.call-done, bf16[2048,1408]{0,1:T(8,128)(2,1)} %all-gather.6.cloned.1.call-done, f32[512,704]{0,1:T(8,128)} %fusion.4, f32[512,2048]{1,0:T(8,128)} %bitcast.58, f32[2048]{0:T(1024)S(1)} %copy-done.4, ...), kind=kOutput, calls=%fused_computation.11 | convolution fusion | flops 2959147008 | bytes 13510656 | tf_op jit(solution)/shard_map/dot_general | solution.py:105
  289.0 41.4 %all_to_all.32 = bf16[8,512,256]{2,1,0:T(8,128)(2,1)S(1)} all-to-all(bf16[8,512,256]{2,1,0:T(8,128)(2,1)S(1)} %bitcast.55), channel_id=1, replica_groups=mesh['grp'=2,'fs'=16,'tp'=8] {'tp'}, dimensions={0} | all-to-all | bytes 4194304 | tf_op jit(solution)/shard_map/all_to_all | solution.py:39
  331.5 4.3 %all-to-all-start.5 = ((f32[8,1,512]{2,1,0:T(1,128)}), f32[8,1,512]{2,1,0:T(1,128)S(1)}, u32[]{:S(2)}, u32[]{:S(2)}) async-start(f32[8,1,512]{2,1,0:T(1,128)} %broadcast_in_dim.24), calls=%async_computation.5 | async-start | bytes 32768 | tf_op jit(solution)/shard_map/all_to_all | solution.py:15
  336.6 4.0 %all-to-all-done.5 = f32[8,1,512]{2,1,0:T(1,128)S(1)} async-done(((f32[8,1,512]{2,1,0:T(1,128)}), f32[8,1,512]{2,1,0:T(1,128)S(1)}, u32[]{:S(2)}, u32[]{:S(2)}) %all-to-all-start.5) | async-done | bytes 16416 | tf_op jit(solution)/shard_map/all_to_all | solution.py:15
  (41 shorter events, 9.5 us)
Async XLA Ops:
  6.5 30.1 %copy-start = (f32[3,1024]{1,0:T(4,128)S(1)}, f32[3,1024]{1,0:T(4,128)}, u32[]{:S(2)}) copy-start(f32[3,1024]{1,0:T(4,128)} %param.17) | copy-start | bytes 36868
  6.6 91.9 %all-gather.4.cloned.1.call-start = ((), (), s32[]{:S(2)}) async-start(), calls=%async_computation.6 | async-start | bytes 1671168 | tf_op jit(solution)/shard_map/all_gather | solution.py:24
  8.1 192.4 %all-gather.6.cloned.1.call-start = ((), (), s32[]{:S(2)}) async-start(), calls=%async_computation.7 | async-start | bytes 6127616 | tf_op jit(solution)/shard_map/all_gather | solution.py:24
  12.5 24.1 %copy-start.2 = (bf16[128,128]{1,0:T(8,128)(2,1)S(1)}, bf16[128,128]{1,0:T(8,128)(2,1)}, u32[]{:S(2)}) copy-start(bf16[128,128]{1,0:T(8,128)(2,1)} %param.18) | copy-start | bytes 98308
  12.5 50.4 %all-to-all-start = ((bf16[8,4,128,256]{3,2,1,0:T(8,128)(2,1)}), bf16[8,4,128,256]{3,2,1,0:T(8,128)(2,1)S(1)}, u32[]{:S(2)}, u32[]{:S(2)}) async-start(bf16[8,4,128,256]{3,2,1,0:T(8,128)(2,1)} %broadcast_in_dim.20), calls=%async_computation | async-start | bytes 4194304 | tf_op jit(solution)/shard_map/all_to_all | solution.py:15
  63.7 38.3 %all-to-all-start.1 = ((bf16[16,128,128]{1,2,0:T(8,128)(2,1)}), bf16[16,128,128]{1,2,0:T(8,128)(2,1)S(1)}, u32[]{:S(2)}, u32[]{:S(2)}) async-start(bf16[16,128,128]{1,2,0:T(8,128)(2,1)} %broadcast_in_dim.21), calls=%async_computation.1 | async-start | bytes 1048576 | tf_op jit(solution)/shard_map/all_to_all | solution.py:15
  74.4 0.7 copy-start.3
  109.8 39.2 %all-to-all-start.2 = ((bf16[8,512,256]{2,1,0:T(8,128)(2,1)}), bf16[8,512,256]{2,1,0:T(8,128)(2,1)S(1)}, u32[]{:S(2)}, u32[]{:S(2)}) async-start(bf16[8,512,256]{2,1,0:T(8,128)(2,1)} %bitcast.53), calls=%async_computation.2 | async-start | bytes 4194304 | tf_op jit(solution)/shard_map/all_to_all | solution.py:39
  122.9 26.5 %copy-start.1 = (bf16[4,128,256]{2,1,0:T(8,128)(2,1)S(1)}, bf16[4,128,256]{2,1,0:T(8,128)(2,1)}, u32[]{:S(2)}) copy-start(bf16[4,128,256]{2,1,0:T(8,128)(2,1)} %param.12) | copy-start | bytes 786436
  122.9 158.1 %all-gather.8.cloned.1.call-start = ((), (), s32[]{:S(2)}) async-start(), calls=%async_computation.8 | async-start | bytes 3063808 | tf_op jit(solution)/shard_map/all_gather | solution.py:107
  186.3 14.1 %copy-start.4 = (f32[2048]{0:T(1024)S(1)}, f32[2048]{0:T(1024)}, u32[]{:S(2)}) copy-start(f32[2048]{0:T(1024)} %param.19) | copy-start | bytes 24580
  331.5 9.0 %all-to-all-start.5 = ((f32[8,1,512]{2,1,0:T(1,128)}), f32[8,1,512]{2,1,0:T(1,128)S(1)}, u32[]{:S(2)}, u32[]{:S(2)}) async-start(f32[8,1,512]{2,1,0:T(1,128)} %broadcast_in_dim.24), calls=%async_computation.5 | async-start | bytes 32768 | tf_op jit(solution)/shard_map/all_to_all | solution.py:15
Sparse Core Ops, SparseCore 0:
  9.1 89.2 all-gather.3
  100.2 100.1 all-gather.5
  202.2 78.7 all-gather.7
where the time goes:
time: 349 us; the launch traced here: 348 us
  waiting for transfers between devices  168 us (48%)
  blocking collectives  71.1 us (20%)
  starting transfers between devices  47.1 us (13%)
  matrix products  22 us (6%)
  local copies, waits for them, and re-layouts  19.4 us (6%)
  between operations  13.3 us (4%)
  other arithmetic  7.44 us (2%)
    all_gather x1, waiting for transfers between devices, local(): lax.all_gather(ffn_down, 'fs', axis=1, tiled=True)  74.6 us
    all_to_all x1, blocking collectives, summed_on_arrival(): lax.all_to_all(parts, axis, split_axis=0, concat_axis=0, tiled=True)  41.4 us
    all_gather x2, waiting for transfers between devices, side_by_side(): filled, at, outs = (lax.all_gather(both, axis, axis=dim, tiled=True), 0, [])  36.6 us
    all_to_all x3, starting transfers between devices, copy_for_each(): return lax.all_to_all(copies, axis, split_axis=0, concat_axis=0, tiled=True)  34 us
    all_to_all x3, waiting for transfers between devices, copy_for_each(): return lax.all_to_all(copies, axis, split_axis=0, concat_axis=0, tiled=True)  30.1 us
    all_to_all x1, blocking collectives, copy_for_each(): return lax.all_to_all(copies, axis, split_axis=0, concat_axis=0, tiled=True)  29.7 us
    all_to_all x1, waiting for transfers between devices, summed_on_arrival(): lax.all_to_all(parts, axis, split_axis=0, concat_axis=0, tiled=True)  25.4 us
    all_to_all x1, starting transfers between devices, summed_on_arrival(): lax.all_to_all(parts, axis, split_axis=0, concat_axis=0, tiled=True)  13 us
  transfers between devices with their start and end apart: 7, of which 6 were waited for; matrix products, arithmetic and copies ran while one was open for 11% of the time, Pallas kernels for 0%

commit v1 on v0

--- a/solution.py
+++ b/solution.py
@@ -2,6 +2,13 @@
 import jax.numpy as jnp
 from jax import lax
 from jax.sharding import PartitionSpec as P
+
+
+def gather_over(x, axis, dim):
+    n_dev = lax.axis_size(axis)
+    blocks = jnp.stack([x for _ in range(n_dev)])
+    blocks = lax.all_to_all(blocks, axis, split_axis=0, concat_axis=0)
+    return jnp.concatenate(blocks, axis=dim)
 
 
 def in_order(parts, dim):
@@ -102,11 +109,7 @@
     gate = jnp.dot(sliced, pieces[0], preferred_element_type=jnp.float32)
     upward = jnp.dot(sliced, pieces[1], preferred_element_type=jnp.float32)
     hidden = (jax.nn.silu(gate) * upward).astype(jnp.bfloat16)
-    down_terms = jnp.dot(
-        hidden,
-        lax.all_gather(ffn_down, "fs", axis=1, tiled=True),
-        preferred_element_type=jnp.float32,
-    )
+    down_terms = jnp.dot(hidden, gather_over(ffn_down, "fs", 1), preferred_element_type=jnp.float32)
     down_summed = summed_on_arrival(down_terms.astype(jnp.bfloat16), "tp", 1)
     second = first.astype(jnp.float32) + down_summed
     squares = of_everyone(jnp.sum(second * second, axis=1), "tp")

time: 349 us -> 445 us (1.28)
  waiting for transfers between devices: 168 us -> 258 us
    all_gather x2, waiting for transfers between devices: 36.6 us -> 203 us  [side_by_side(): filled, at, outs = (lax.all_gather(both, axis, axis=dim, tiled=True), 0, [])]
    all_gather x1 -> x0, waiting for transfers between devices: 74.6 us -> none  [local(): lax.all_gather(ffn_down, 'fs', axis=1, tiled=True)]
    all_to_all x1 -> x2, blocking collectives: 41.4 us -> 75.4 us  [summed_on_arrival(): lax.all_to_all(parts, axis, split_axis=0, concat_axis=0, tiled=True)]
    all_to_all x1 -> x0, blocking collectives: 29.7 us -> none  [copy_for_each(): return lax.all_to_all(copies, axis, split_axis=0, concat_axis=0, tiled=True)]
    all_to_all x1, waiting for transfers between devices: 25.4 us -> 0.01 us  [gather_over(): blocks = lax.all_to_all(blocks, axis, split_axis=0, concat_axis=0)]
    all_to_all x3 -> x4, waiting for transfers between devices: 30.1 us -> 54.8 us  [copy_for_each(): return lax.all_to_all(copies, axis, split_axis=0, concat_axis=0, tiled=True)]
    all_to_all x1, starting transfers between devices: 13 us -> 8.13 us  [gather_over(): blocks = lax.all_to_all(blocks, axis, split_axis=0, concat_axis=0)]
    all_to_all x3 -> x4, starting transfers between devices: 34 us -> 38.7 us  [copy_for_each(): return lax.all_to_all(copies, axis, split_axis=0, concat_axis=0, tiled=True)]
  transfers between devices with their start and end apart: 7 -> 7, of which waited for: 6 -> 5; matrix products, arithmetic and copies ran while one was open for 11% -> 6% of each run, Pallas kernels for 0% -> 0%
where the time goes in v1:
time: 445 us; the launch traced here: 444 us
  waiting for transfers between devices  258 us (58%)
  blocking collectives  75.4 us (17%)
  starting transfers between devices  46.9 us (11%)
  local copies, waits for them, and re-layouts  22.1 us (5%)
  matrix products  22 us (5%)
  between operations  13.7 us (3%)
  other arithmetic  5.61 us (1%)
    all_gather x2, waiting for transfers between devices, side_by_side(): filled, at, outs = (lax.all_gather(both, axis, axis=dim, tiled=True), 0, [])  203 us
    all_to_all x2, blocking collectives, summed_on_arrival(): lax.all_to_all(parts, axis, split_axis=0, concat_axis=0, tiled=True)  75.4 us
    all_to_all x4, waiting for transfers between devices, copy_for_each(): return lax.all_to_all(copies, axis, split_axis=0, concat_axis=0, tiled=True)  54.8 us
    all_to_all x4, starting transfers between devices, copy_for_each(): return lax.all_to_all(copies, axis, split_axis=0, concat_axis=0, tiled=True)  38.7 us
  transfers between devices with their start and end apart: 7, of which 5 were waited for; matrix products, arithmetic and copies ran while one was open for 6% of the time, Pallas kernels for 0%

profile of v1, /device:TPU:33, one launch (start us, length us, event | category | flops | bytes accessed | tf_op | source)
XLA Modules:
  0.0 443.9 jit_solution(6071463160645724557)
XLA Ops:
  6.6 2.5 broadcast_in_dim.20
  9.1 24.1 %all-to-all-start = ((bf16[8,4,128,256]{3,2,1,0:T(8,128)(2,1)}), bf16[8,4,128,256]{3,2,1,0:T(8,128)(2,1)S(1)}, u32[]{:S(2)}, u32[]{:S(2)}) async-start(bf16[8,4,128,256]{3,2,1,0:T(8,128)(2,1)} %broadcast_in_dim.20), calls=%async_computation | async-start | bytes 4194304 | tf_op jit(solution)/shard_map/all_to_all | solution.py:22
  34.1 25.4 %all-to-all-done = bf16[8,4,128,256]{3,2,1,0:T(8,128)(2,1)S(1)} async-done(((bf16[8,4,128,256]{3,2,1,0:T(8,128)(2,1)}), bf16[8,4,128,256]{3,2,1,0:T(8,128)(2,1)S(1)}, u32[]{:S(2)}, u32[]{:S(2)}) %all-to-all-start) | async-done | bytes 2097184 | tf_op jit(solution)/shard_map/all_to_all | solution.py:22
  60.4 5.7 %all-to-all-start.1 = ((bf16[16,128,128]{1,2,0:T(8,128)(2,1)}), bf16[16,128,128]{1,2,0:T(8,128)(2,1)S(1)}, u32[]{:S(2)}, u32[]{:S(2)}) async-start(bf16[16,128,128]{1,2,0:T(8,128)(2,1)} %broadcast_in_dim.21), calls=%async_computation.1 | async-start | bytes 1048576 | tf_op jit(solution)/shard_map/all_to_all | solution.py:22
  66.6 2.4 copy.26
  69.0 2.0 copy.37
  72.1 35.0 %all-gather.3.cloned.1.call-done = bf16[2048,384]{1,0:T(8,128)(2,1)} async-done(((bf16[128,384]{1,0:T(8,128)(2,1)}), bf16[2048,384]{1,0:T(8,128)(2,1)}) %all-gather.3.cloned.1.call-update) | async-done | bytes 1572880 | tf_op jit(solution)/shard_map/all_gather | solution.py:31
  107.1 1.7 fusion.16
  108.8 1.8 fusion.15
  110.7 4.7 %convolution_convert_fusion = bf16[512,2048]{1,0:T(8,128)(2,1)} fusion(bf16[128,2048]{0,1:T(8,128)(2,1)S(1)} %bitcast.68, f32[512,128]{1,0:T(8,128)S(1)} %bitcast.70, bf16[512,2048]{1,0:T(8,128)(2,1)S(1)} %multiply_convert_fusion.1, bf16[2048,384]{1,0:T(8,128)(2,1)} %all-gather.3.cloned.1.call-done), kind=kOutput, calls=%fused_computation.10 | convolution fusion | flops 538181632 | bytes 5505024 | tf_op jit(solution)/shard_map/dot_general | solution.py:98
  115.4 1.7 copy.46
  117.1 37.0 %all_to_all.36 = bf16[8,512,256]{2,1,0:T(8,128)(2,1)S(1)} all-to-all(bf16[8,512,256]{2,1,0:T(8,128)(2,1)S(1)} %bitcast.61), channel_id=1, replica_groups=mesh['grp'=2,'fs'=16,'tp'=8] {'tp'}, dimensions={0} | all-to-all | bytes 4194304 | tf_op jit(solution)/shard_map/all_to_all | solution.py:46
  156.7 4.7 %all-to-all-start.3 = ((bf16[8,4,128,256]{3,2,1,0:T(8,128)(2,1)}), bf16[8,4,128,256]{3,2,1,0:T(8,128)(2,1)S(1)}, u32[]{:S(2)}, u32[]{:S(2)}) async-start(bf16[8,4,128,256]{3,2,1,0:T(8,128)(2,1)} %broadcast_in_dim.22), calls=%async_computation.3 | async-start | bytes 4194304 | tf_op jit(solution)/shard_map/all_to_all | solution.py:22
  162.3 25.5 %all-to-all-done.3 = bf16[8,4,128,256]{3,2,1,0:T(8,128)(2,1)S(1)} async-done(((bf16[8,4,128,256]{3,2,1,0:T(8,128)(2,1)}), bf16[8,4,128,256]{3,2,1,0:T(8,128)(2,1)S(1)}, u32[]{:S(2)}, u32[]{:S(2)}) %all-to-all-start.3) | async-done | bytes 2097184 | tf_op jit(solution)/shard_map/all_to_all | solution.py:22
  187.7 2.1 stack.2
  189.8 8.1 %all-to-all-start.4 = ((bf16[16,704,128]{2,1,0:T(8,128)(2,1)}), bf16[16,704,128]{2,1,0:T(8,128)(2,1)}, u32[]{:S(2)}, u32[]{:S(2)}) async-start(bf16[16,704,128]{2,1,0:T(8,128)(2,1)} %stack.2), calls=%async_computation.4 | async-start | bytes 5767168 | tf_op jit(solution)/shard_map/all_to_all | solution.py:10
  198.5 2.4 copy.29
  200.9 4.0 copy.38
  205.4 168.4 %all-gather.5.cloned.1.call-done = bf16[2048,1408]{0,1:T(8,128)(2,1)} async-done(((bf16[128,1408]{0,1:T(8,128)(2,1)}), bf16[2048,1408]{0,1:T(8,128)(2,1)}) %all-gather.5.cloned.1.call-update) | async-done | bytes 5767184 | tf_op jit(solution)/shard_map/all_gather | solution.py:31
  373.8 6.0 %fusion.6 = f32[512,704]{0,1:T(8,128)} fusion(bf16[2048,1408]{0,1:T(8,128)(2,1)} %all-gather.5.cloned.1.call-done, f32[512,2048]{1,0:T(8,128)} %bitcast.64, f32[2048]{0:T(1024)S(1)} %copy-done.11, f32[512]{0:T(512)S(1)} %rsqrt_bitcast_fusion.1), kind=kOutput, calls=%fused_computation.16 | convolution fusion | flops 1479540736 | bytes 8529920 | tf_op jit(solution)/shard_map/dot_general | solution.py:109
  379.8 7.8 %convolution_convert_fusion.1 = bf16[512,2048]{1,0:T(8,128)(2,1)S(1)} fusion(bf16[2048,1408]{0,1:T(8,128)(2,1)} %all-gather.5.cloned.1.call-done, f32[512,704]{0,1:T(8,128)} %fusion.6, f32[512,2048]{1,0:T(8,128)} %bitcast.65, f32[2048]{0:T(1024)S(1)} %copy-done.11, f32[512]{0:T(512)S(1)} %rsqrt_bitcast_fusion.1, bf16[16,704,128]{2,1,0:T(8,128)(2,1)} %all-to-all-done.4), kind=kOutput, calls=%fused_computation.11 | convolution fusion | flops 2959147008 | bytes 13510656 | tf_op jit(solution)/shard_map/dot_general | solution.py:112
  387.8 38.3 %all_to_all.37 = bf16[8,512,256]{2,1,0:T(8,128)(2,1)S(1)} all-to-all(bf16[8,512,256]{2,1,0:T(8,128)(2,1)S(1)} %bitcast.62), channel_id=1, replica_groups=mesh['grp'=2,'fs'=16,'tp'=8] {'tp'}, dimensions={0} | all-to-all | bytes 4194304 | tf_op jit(solution)/shard_map/all_to_all | solution.py:46
  427.2 4.3 all-to-all-start.6
  432.2 4.0 all-to-all-done.6
  (55 shorter events, 10.7 us)
Async XLA Ops:
  6.5 27.5 %copy-start = (f32[3,1024]{1,0:T(4,128)S(1)}, f32[3,1024]{1,0:T(4,128)}, u32[]{:S(2)}) copy-start(f32[3,1024]{1,0:T(4,128)} %param.17) | copy-start | bytes 36868
  9.1 24.1 %copy-start.7 = (bf16[128,128]{1,0:T(8,128)(2,1)S(1)}, bf16[128,128]{1,0:T(8,128)(2,1)}, u32[]{:S(2)}) copy-start(bf16[128,128]{1,0:T(8,128)(2,1)} %param.16) | copy-start | bytes 98308
  9.1 24.1 %copy-start.8 = (bf16[128,128]{1,0:T(8,128)(2,1)S(1)}, bf16[128,128]{1,0:T(8,128)(2,1)}, u32[]{:S(2)}) copy-start(bf16[128,128]{1,0:T(8,128)(2,1)} %param.15) | copy-start | bytes 98308
  9.1 24.1 %copy-start.9 = (bf16[128,128]{1,0:T(8,128)(2,1)S(1)}, bf16[128,128]{1,0:T(8,128)(2,1)}, u32[]{:S(2)}) copy-start(bf16[128,128]{1,0:T(8,128)(2,1)} %param.14) | copy-start | bytes 98308
  9.1 24.8 %copy-start.6 = (bf16[128,128]{1,0:T(8,128)(2,1)S(1)}, bf16[128,128]{1,0:T(8,128)(2,1)}, u32[]{:S(2)}) copy-start(bf16[128,128]{1,0:T(8,128)(2,1)} %param.18) | copy-start | bytes 98308
  9.1 50.4 %all-to-all-start = ((bf16[8,4,128,256]{3,2,1,0:T(8,128)(2,1)}), bf16[8,4,128,256]{3,2,1,0:T(8,128)(2,1)S(1)}, u32[]{:S(2)}, u32[]{:S(2)}) async-start(bf16[8,4,128,256]{3,2,1,0:T(8,128)(2,1)} %broadcast_in_dim.20), calls=%async_computation | async-start | bytes 4194304 | tf_op jit(solution)/shard_map/all_to_all | solution.py:22
  33.2 73.9 %all-gather.3.cloned.1.call-start = ((), (), s32[]{:S(2)}) async-start(), calls=%async_computation.7 | async-start | bytes 1671168 | tf_op jit(solution)/shard_map/all_gather | solution.py:31
  60.4 50.3 %all-to-all-start.1 = ((bf16[16,128,128]{1,2,0:T(8,128)(2,1)}), bf16[16,128,128]{1,2,0:T(8,128)(2,1)S(1)}, u32[]{:S(2)}, u32[]{:S(2)}) async-start(bf16[16,128,128]{1,2,0:T(8,128)(2,1)} %broadcast_in_dim.21), calls=%async_computation.1 | async-start | bytes 1048576 | tf_op jit(solution)/shard_map/all_to_all | solution.py:22
  71.0 0.7 copy-start.10
  154.2 1.0 copy-start.2
  156.7 4.7 %copy-start.3 = (bf16[128,704]{0,1:T(8,128)(2,1)S(1)}, bf16[128,704]{0,1:T(8,128)(2,1)}, u32[]{:S(2)}) copy-start(bf16[128,704]{0,1:T(8,128)(2,1)} %param.21) | copy-start | bytes 540676
  156.7 4.7 %copy-start.4 = (bf16[128,704]{0,1:T(8,128)(2,1)S(1)}, bf16[128,704]{0,1:T(8,128)(2,1)}, u32[]{:S(2)}) copy-start(bf16[128,704]{0,1:T(8,128)(2,1)} %param.20) | copy-start | bytes 540676
  156.7 31.0 %copy-start.5 = (bf16[704,128]{1,0:T(8,128)(2,1)S(1)}, bf16[704,128]{1,0:T(8,128)(2,1)}, u32[]{:S(2)}) copy-start(bf16[704,128]{1,0:T(8,128)(2,1)} %param.22) | copy-start | bytes 540676
  156.7 31.0 %all-to-all-start.3 = ((bf16[8,4,128,256]{3,2,1,0:T(8,128)(2,1)}), bf16[8,4,128,256]{3,2,1,0:T(8,128)(2,1)S(1)}, u32[]{:S(2)}, u32[]{:S(2)}) async-start(bf16[8,4,128,256]{3,2,1,0:T(8,128)(2,1)} %broadcast_in_dim.22), calls=%async_computation.3 | async-start | bytes 4194304 | tf_op jit(solution)/shard_map/all_to_all | solution.py:22
  161.4 212.4 %all-gather.5.cloned.1.call-start = ((), (), s32[]{:S(2)}) async-start(), calls=%async_computation.8 | async-start | bytes 6127616 | tf_op jit(solution)/shard_map/all_gather | solution.py:31
  189.8 189.9 %all-to-all-start.4 = ((bf16[16,704,128]{2,1,0:T(8,128)(2,1)}), bf16[16,704,128]{2,1,0:T(8,128)(2,1)}, u32[]{:S(2)}, u32[]{:S(2)}) async-start(bf16[16,704,128]{2,1,0:T(8,128)(2,1)} %stack.2), calls=%async_computation.4 | async-start | bytes 5767168 | tf_op jit(solution)/shard_map/all_to_all | solution.py:10
  204.9 168.9 %copy-start.11 = (f32[2048]{0:T(1024)S(1)}, f32[2048]{0:T(1024)}, u32[]{:S(2)}) copy-start(f32[2048]{0:T(1024)} %param.19) | copy-start | bytes 24580
  387.8 49.3 %copy-start.1 = (f32[3,1024]{1,0:T(4,128)S(1)}, f32[3,1024]{1,0:T(4,128)}, u32[]{:S(2)}) copy-start(f32[3,1024]{1,0:T(4,128)} %param.17) | copy-start | bytes 36868
  427.2 9.0 %all-to-all-start.6 = ((f32[8,1,512]{2,1,0:T(1,128)}), f32[8,1,512]{2,1,0:T(1,128)S(1)}, u32[]{:S(2)}, u32[]{:S(2)}) async-start(f32[8,1,512]{2,1,0:T(1,128)} %broadcast_in_dim.24), calls=%async_computation.6 | async-start | bytes 32768 | tf_op jit(solution)/shard_map/all_to_all | solution.py:22
Sparse Core Ops, SparseCore 0:
  35.8 71.2 all-gather.2
  164.0 209.8 all-gather.4
